TPU v7x, 32 devices: a whole 2x2x4 slice. The times are simulated.
32 devices in a mesh: sp: 16 (over z, y, x), tp: 2 (over core).
Axes of the slice: x: 2, y: 2, z: 4, core: 2. Of those that a mesh axis runs over, the one named last changes fastest.
Arguments:
- queries: bfloat16 [8192, 8, 128], P('sp', 'tp'), may hold values from -60 to 60
- keys: bfloat16 [8192, 8, 128], P('sp', 'tp'), may hold values from -40 to 40
- values: bfloat16 [8192, 8, 128], P('sp', 'tp'), may hold values from -6 to 6
- w_out: bfloat16 [1024, 2048], P(None, 'tp'), may hold values from -0.1875 to 0.1875
Outputs:
- mixed: bfloat16 [8192, 2048], P('sp', 'tp')
All inputs are finite; a program needn't handle non-finite values.
Results may differ from a plain program's by a relative error of at most 0.0051.
Values may be sent and summed in bfloat16 or wider, within the bound.
A program may use at most 64 MiB of HBM per device.

v0:
```python
import functools
import math

import jax
import jax.numpy as jnp
from jax import lax
from jax.experimental import pallas as pl
from jax.experimental.pallas import tpu as pltpu
from jax.sharding import PartitionSpec as P

W1 = 128
WINDOW_TWO = 512
DILATION_TWO = 4
WINDOW_THREE = 2048
DILATION_THREE = 16
MESH = pl.DeviceIdType.MESH
RATIO = DILATION_THREE // DILATION_TWO
CHUNKS = DILATION_TWO
ROWS_ONE = 16
ROWS_TWO = WINDOW_TWO // DILATION_THREE


def attend(blocks, scale):
    scores = [
        lax.dot_general(q, k, (((1,), (1,)), ((), ())), preferred_element_type=jnp.float32)
        for q, k, _, _ in blocks
    ]
    scores = [x * scale + bias for x, (_, _, _, bias) in zip(scores, blocks)]
    tops = [jnp.max(x, axis=-1, keepdims=True) for x in scores]
    numerators = [jnp.exp2(x - top) for x, top in zip(scores, tops)]
    sums = [
        jnp.dot(
            x.astype(v.dtype), jnp.concatenate([v, jnp.ones_like(v)], axis=1), preferred_element_type=jnp.float32
        )
        for x, (_, _, v, _) in zip(numerators, blocks)
    ]
    dim = blocks[0][2].shape[-1]
    return [(x[:, :dim], jnp.broadcast_to(top, x[:, :dim].shape), x[:, dim:]) for x, top in zip(sums, tops)]


def bias_of(shape, place_q, place_k, first_own, window, has_prev):
    query_place, _ = place_q(lax.broadcasted_iota(jnp.int32, shape, 0))
    key_place, key_row = place_k(lax.broadcasted_iota(jnp.int32, shape, 1))
    distance = query_place - key_place
    allowed = (distance >= 0) & (distance <= window)
    general = jnp.where(allowed, 0.0, -jnp.inf).astype(jnp.float32)
    gate = jnp.where(has_prev, 0, first_own)
    first = jnp.where(allowed & (key_row >= gate), 0.0, -jnp.inf).astype(jnp.float32)
    return general, first


def kernel(
    group, q_ref, k_ref, v_ref, w_ref, o_ref,
    qb, kb, vb, acc, mx, sm, ob, ab, bias1, bias1f, bias2, bias2f, bias3,
    in_send, in_recv, z_send, z_recv, zl_send, zl_recv, o_send, o_recv, d_send, d_recv,
):
    res, dim = DILATION_THREE, q_ref.shape[-1]
    piece = q_ref.shape[2]
    rows = group * piece
    sp, tp = lax.axis_index("sp"), lax.axis_index("tp")
    n_sp, n_tp = lax.axis_size("sp"), lax.axis_size("tp")
    mine = lax.rem(sp, group)
    base = sp - mine
    has_prev = sp >= group
    has_next = sp + group < n_sp
    partner = n_tp - 1 - tp
    scale = math.log2(math.e) / math.sqrt(dim)

    barrier = pltpu.get_barrier_semaphore()
    for d in range(1, group):
        pl.semaphore_signal(
            barrier, inc=1, device_id={"sp": base + lax.rem(mine + d, group)}, device_id_type=MESH
        )
    pl.semaphore_signal(barrier, inc=1, device_id={"tp": partner}, device_id_type=MESH)

    @pl.when(has_prev)
    def _():
        pl.semaphore_signal(barrier, inc=1, device_id={"sp": sp - group}, device_id_type=MESH)

    @pl.when(has_next)
    def _():
        pl.semaphore_signal(barrier, inc=1, device_id={"sp": sp + group}, device_id_type=MESH)

    pl.semaphore_wait(barrier, group + jnp.where(has_prev, 1, 0) + jnp.where(has_next, 1, 0))

    def span(start):
        return pl.ds(pl.multiple_of(start, piece), piece)

    tensors = ((k_ref, kb, rows), (v_ref, vb, rows), (q_ref, qb, 0))

    def member(d):
        other, bit = mine, 1
        while bit <= d:
            if d & bit:
                other = other + bit * (1 - 2 * lax.rem(mine // bit, 2))
            bit *= 2
        return other

    def exchange(which, d):
        source, buffer, offset = tensors[which]
        other = member(d)
        return pltpu.make_async_remote_copy(
            src_ref=source.at[other],
            dst_ref=buffer.at[:, span(offset + piece * mine), :],
            send_sem=in_send.at[which, d],
            recv_sem=in_recv.at[which, d],
            device_id={"sp": base + other},
            device_id_type=MESH,
        )

    def arrival(which, d):
        source, buffer, offset = tensors[which]
        return pltpu.make_async_remote_copy(
            src_ref=source.at[0],
            dst_ref=buffer.at[:, span(offset + piece * member(d)), :],
            send_sem=in_send.at[which, d],
            recv_sem=in_recv.at[which, d],
            device_id={"sp": sp},
            device_id_type=MESH,
        )

    low = piece - ROWS_ONE

    def onward_rows(which, k):
        source, buffer, _ = tensors[which]
        start = piece * member(k)
        if k == 0:
            src, dst = source.at[mine], buffer.at[:, span(start), :]
        elif k in whole:
            src, dst = buffer.at[:, span(rows + start), :], buffer.at[:, span(start), :]
        else:
            ends = [pl.ds(pl.multiple_of(x + start + low, ROWS_ONE), ROWS_ONE) for x in (rows, 0)]
            src, dst = (buffer.at[:, x, :] for x in ends)
        return pltpu.make_async_remote_copy(
            src_ref=src,
            dst_ref=dst,
            send_sem=z_send.at[which, k],
            recv_sem=z_recv.at[which, k],
            device_id={"sp": sp + group},
            device_id_type=MESH,
        )

    def onward_chunk(which, k, s):
        _, buffer, _ = tensors[which]
        start = piece * member(k)
        part = pl.ds(s * RATIO, RATIO)
        return pltpu.make_async_remote_copy(
            src_ref=buffer.at[part, pl.ds(pl.multiple_of(rows + start, ROWS_ONE), low), :],
            dst_ref=buffer.at[part, pl.ds(pl.multiple_of(start, ROWS_ONE), low), :],
            send_sem=zl_send.at[which, k, s],
            recv_sem=zl_recv.at[which, k, s],
            device_id={"sp": sp + group},
            device_id_type=MESH,
        )

    whole = range(group // 2)
    split = range(group // 2, group)

    @pl.when(has_next)
    def _():
        for which in (0, 1):
            onward_rows(which, 0).start()

    near = [d for d in range(1, group) if d & (d - 1) == 0]
    far = [d for d in range(1, group) if d & (d - 1)]
    for tensors_now in ((0, 1), (2,)):
        for members in (near, far):
            for which in tensors_now:
                for d in members:
                    exchange(which, d).start()

    for source, buffer, offset in tensors:
        buffer[:, span(offset + piece * mine), :] = source[mine]

    @pl.when(jnp.logical_not(has_prev))
    def _():
        kb[:, :rows, :] = jnp.zeros((res, rows, dim), kb.dtype)
        vb[:, :rows, :] = jnp.zeros((res, rows, dim), vb.dtype)

    def place_one(per):
        def place(i):
            store, row = i // per, i % per
            residue = (store % RATIO) * DILATION_TWO + store // RATIO
            return row * res + residue, row
        return place

    def place_two(per):
        def place(i):
            j, row = i // per, i % per
            return row * RATIO + j, row
        return place

    def shifted(place, by):
        def moved(i):
            at, row = place(i)
            return at + by, row
        return moved

    bias1[...], bias1f[...] = bias_of(
        bias1.shape, shifted(place_one(ROWS_ONE), ROWS_ONE * res), place_one(2 * ROWS_ONE), ROWS_ONE, W1, has_prev
    )
    bias2[...], bias2f[...] = bias_of(
        bias2.shape, shifted(place_two(ROWS_TWO), ROWS_TWO * RATIO), place_two(2 * ROWS_TWO), ROWS_TWO,
        WINDOW_TWO // DILATION_TWO, has_prev,
    )
    _, bias3[...] = bias_of(
        bias3.shape, lambda i: (i + rows, i), lambda i: (i, i), rows, WINDOW_THREE // DILATION_THREE, has_prev
    )

    for k in range(1, group):
        for which in (0, 1):
            arrival(which, k).wait_recv()

        @pl.when(has_next)
        def _():
            for which in (0, 1):
                onward_rows(which, k).start()

    @pl.when(has_next)
    def _():
        for s in range(CHUNKS):
            for k in split:
                for which in (0, 1):
                    onward_chunk(which, k, s).start()

    def branch_one(blocks, bias):
        spans = [
            (
                pl.ds(pl.multiple_of(b * ROWS_ONE, ROWS_ONE), ROWS_ONE),
                pl.ds(pl.multiple_of(rows + (b - 1) * ROWS_ONE, ROWS_ONE), 2 * ROWS_ONE),
            )
            for b in blocks
        ]
        found = attend(
            [
                tuple(x[:, at, :].reshape(-1, dim) for x, at in ((qb, own), (kb, near), (vb, near))) + (bias[...],)
                for own, near in spans
            ],
            scale,
        )
        for (own, _), (weighted, top, total) in zip(spans, found):
            acc[:, own, :] = weighted.reshape(res, ROWS_ONE, dim)
            mx[:, own, :] = top.reshape(res, ROWS_ONE, dim)
            sm[:, own, :] = total.reshape(res, ROWS_ONE, dim)

    def merge(at, weighted, top, total):
        old_top = mx[at].reshape(-1, dim)
        new_top = jnp.maximum(old_top, top)
        old_part, part = jnp.exp2(old_top - new_top), jnp.exp2(top - new_top)
        return (
            acc[at].reshape(-1, dim) * old_part + weighted * part,
            new_top,
            sm[at].reshape(-1, dim) * old_part + total * part,
        )

    def branch_two(blocks, bias):
        spans = [
            (
                pl.ds(s * RATIO, RATIO),
                pl.ds(b * ROWS_TWO, ROWS_TWO),
                pl.ds(rows + (b - 1) * ROWS_TWO, 2 * ROWS_TWO),
            )
            for s, b in blocks
        ]
        found = attend(
            [
                tuple(x[part, at, :].reshape(-1, dim) for x, at in ((qb, own), (kb, near), (vb, near))) + (bias[...],)
                for part, own, near in spans
            ],
            scale,
        )
        merged = [merge((part, own, slice(None)), *one) for (part, own, _), one in zip(spans, found)]
        for (part, own, _), (weighted, top, total) in zip(spans, merged):
            acc[part, own, :] = weighted.reshape(RATIO, ROWS_TWO, dim)
            mx[part, own, :] = top.reshape(RATIO, ROWS_TWO, dim)
            sm[part, own, :] = total.reshape(RATIO, ROWS_TWO, dim)

    def some(items, count):
        return [items[i : i + count] for i in range(0, len(items), count)]

    steps = piece // ROWS_ONE
    for d in [0] + near + far:
        if d:
            arrival(2, d).wait_recv()
        for inner in range(1, steps):
            branch_one([member(d) * steps + inner], bias1)
    for b in range(steps, rows // ROWS_ONE, steps):
        branch_one([b], bias1)
    for blocks in some([(s, b) for s in range(CHUNKS) for b in range(1, rows // ROWS_TWO)], 2):
        branch_two(blocks, bias2)

    @pl.when(has_prev)
    def _():
        for k in range(group):
            for which in (0, 1):
                onward_rows(which, k).wait_recv()

    branch_one([0], bias1f)

    head = tp * group + mine

    def lanes(index):
        return pl.ds(pl.multiple_of(index * dim, dim), dim)

    def give(s, d):
        part = pl.ds(s * RATIO, RATIO)
        other = member(d)
        return pltpu.make_async_remote_copy(
            src_ref=ob.at[part, span(piece * other), :],
            dst_ref=ab.at[part, :, lanes(head)],
            send_sem=o_send.at[s, d],
            recv_sem=o_recv.at[s, d],
            device_id={"sp": base + other},
            device_id_type=MESH,
        )

    def taken(s, d):
        part = pl.ds(s * RATIO, RATIO)
        return pltpu.make_async_remote_copy(
            src_ref=ob.at[part, span(0), :],
            dst_ref=ab.at[part, :, lanes(tp * group + member(d))],
            send_sem=o_send.at[s, d],
            recv_sem=o_recv.at[s, d],
            device_id={"sp": sp},
            device_id_type=MESH,
        )

    def swap(s, d):
        part = pl.ds(s * RATIO, RATIO)
        slot = ab.at[part, :, lanes(tp * group + member(d))]
        return pltpu.make_async_remote_copy(
            src_ref=ob.at[part, span(piece * mine), :] if d == 0 else slot,
            dst_ref=slot,
            send_sem=d_send.at[s, d],
            recv_sem=d_recv.at[s, d],
            device_id={"tp": partner},
            device_id_type=MESH,
        )

    def swapped(s, d):
        part = pl.ds(s * RATIO, RATIO)
        return pltpu.make_async_remote_copy(
            src_ref=ob.at[part, span(0), :],
            dst_ref=ab.at[part, :, lanes(partner * group + member(d))],
            send_sem=d_send.at[s, d],
            recv_sem=d_recv.at[s, d],
            device_id={"tp": partner},
            device_id_type=MESH,
        )

    def hand_over(s):
        for d in range(1, group):
            taken(s, d).wait_recv()
            swap(s, d).start()

    def project(s):
        part = pl.ds(s * RATIO, RATIO)
        for d in range(group):
            swapped(s, d).wait_recv()
        attended = ab[part].reshape(RATIO * piece, -1)
        mixed = jnp.dot(attended, w_ref[...], preferred_element_type=jnp.float32)
        o_ref[part] = mixed.astype(o_ref.dtype).reshape(RATIO, piece, -1)

    for s in range(CHUNKS):
        part = pl.ds(s * RATIO, RATIO)

        @pl.when(has_prev)
        def _():
            for k in split:
                for which in (0, 1):
                    onward_chunk(which, k, s).wait_recv()

        branch_two([(s, 0)], bias2f)
        for stores in some(list(range(s * RATIO, (s + 1) * RATIO)), 2):
            found = attend([(qb[x], kb[x], vb[x], bias3[...]) for x in stores], scale)
            for x, one in zip(stores, found):
                weighted, _, total = merge((x,), *one)
                ob[x] = (weighted / total).astype(ob.dtype)
        for d in far + near:
            give(s, d).start()
        swap(s, 0).start()
        ab[part, :, lanes(head)] = ob[part, span(piece * mine), :]
        if s >= 2:
            hand_over(s - 2)
    for s in range(CHUNKS - 2, CHUNKS):
        hand_over(s)
        project(s - 2)
    for s in range(CHUNKS - 2, CHUNKS):
        project(s)

    for which in (0, 1, 2):
        for d in range(1, group):
            exchange(which, d).wait_send()

    @pl.when(has_next)
    def _():
        for which in (0, 1):
            for k in range(group):
                onward_rows(which, k).wait_send()
            for k in split:
                for s in range(CHUNKS):
                    onward_chunk(which, k, s).wait_send()

    for s in range(CHUNKS):
        for d in range(1, group):
            give(s, d).wait_send()
        for d in range(group):
            swap(s, d).wait_send()


def local(queries, keys, values, w_out):
    tokens, group, dim = queries.shape
    features, columns = w_out.shape
    res = DILATION_THREE
    piece = tokens // res
    rows = group * piece
    assert group & (group - 1) == 0 and piece > ROWS_ONE
    assert group * tokens == WINDOW_THREE and lax.axis_size("sp") % group == 0 and lax.axis_size("tp") == 2

    def by_residue(x):
        x = x.reshape(piece, RATIO, DILATION_TWO, group, dim)
        return jnp.transpose(x, (3, 2, 1, 0, 4)).reshape(group, res, piece, dim)

    low, full = jnp.bfloat16, jnp.float32
    dma = pltpu.SemaphoreType.DMA
    vmem = pl.BlockSpec(memory_space=pltpu.VMEM)
    mixed = pl.pallas_call(
        functools.partial(kernel, group),
        out_shape=jax.ShapeDtypeStruct((res, piece, columns), low),
        in_specs=[vmem] * 4,
        out_specs=vmem,
        scratch_shapes=[
            pltpu.VMEM((res, rows, dim), low),
            pltpu.VMEM((res, 2 * rows, dim), low),
            pltpu.VMEM((res, 2 * rows, dim), low),
            pltpu.VMEM((res, rows, dim), full),
            pltpu.VMEM((res, rows, dim), full),
            pltpu.VMEM((res, rows, dim), full),
            pltpu.VMEM((res, rows, dim), low),
            pltpu.VMEM((res, piece, features), low),
            pltpu.VMEM((res * ROWS_ONE, 2 * res * ROWS_ONE), full),
            pltpu.VMEM((res * ROWS_ONE, 2 * res * ROWS_ONE), full),
            pltpu.VMEM((RATIO * ROWS_TWO, 2 * RATIO * ROWS_TWO), full),
            pltpu.VMEM((RATIO * ROWS_TWO, 2 * RATIO * ROWS_TWO), full),
            pltpu.VMEM((rows, 2 * rows), full),
            dma((3, group)), dma((3, group)),
            dma((2, group)), dma((2, group)),
            dma((2, group, CHUNKS)), dma((2, group, CHUNKS)),
            dma((CHUNKS, group)), dma((CHUNKS, group)),
            dma((CHUNKS, group)), dma((CHUNKS, group)),
        ],
        compiler_params=pltpu.CompilerParams(
            collective_id=0, has_side_effects=True, vmem_limit_bytes=48 * 2**20
        ),
    )(by_residue(queries), by_residue(keys), by_residue(values), w_out)
    mixed = mixed.reshape(DILATION_TWO, RATIO, piece, columns)
    return jnp.transpose(mixed, (2, 1, 0, 3)).reshape(tokens, columns)


def solution(mesh):
    in_specs = (P("sp", "tp", None), P("sp", "tp", None), P("sp", "tp", None), P(None, "tp"))
    out_specs = P("sp", "tp")
    return jax.shard_map(local, mesh=mesh, in_specs=in_specs, out_specs=out_specs, check_vma=False)
```

profile of v0, /device:TPU:0, one launch (start us, length us, event | category | flops | bytes accessed | tf_op | source)
XLA Modules:
  0.0 44.0 jit_solution(1735908423102288559)
XLA Ops:
  0.0 0.0 copy-start
  0.0 1.5 %copy.5 = bf16[32,4,4,4,128]{4,0,1,2,3:T(8,128)(2,1)S(1)} copy(bf16[32,4,4,4,128]{4,3,2,1,0:T(4,128)(2,1)} %bitcast.19) | data formatting | bytes 1048576 | tf_op jit(solution)/shard_map/reshape | solution.py:421
  1.5 1.4 %copy.6 = bf16[32,4,4,4,128]{4,0,1,2,3:T(8,128)(2,1)S(1)} copy(bf16[32,4,4,4,128]{4,3,2,1,0:T(4,128)(2,1)} %bitcast.20) | data formatting | bytes 1048576 | tf_op jit(solution)/shard_map/reshape | solution.py:421
  2.9 1.4 %copy.7 = bf16[32,4,4,4,128]{4,0,1,2,3:T(8,128)(2,1)S(1)} copy(bf16[32,4,4,4,128]{4,3,2,1,0:T(4,128)(2,1)} %bitcast.21) | data formatting | bytes 1048576 | tf_op jit(solution)/shard_map/reshape | solution.py:421
  4.3 0.0 copy-done
  4.3 37.7 %shard_map.46 = bf16[16,32,1024]{2,1,0:T(8,128)(2,1)S(1)} custom-call(bf16[4,16,32,128]{3,2,1,0:T(8,128)(2,1)S(1)} %bitcast.16, bf16[4,16,32,128]{3,2,1,0:T(8,128)(2,1)S(1)} %bitcast.17, bf16[4,16,32,128]{3,2,1,0:T(8,128)(2,1)S(1)} %bitcast.18, bf16[1024,1024]{1,0:T(8,128)(2,1)S(1)} %copy-done), custom_call_target="tpu_custom_call" | custom-call | tf_op jit(solution)/shard_map/pallas_call | solution.py:427
  42.1 0.8 %copy.8 = bf16[32,4,4,1024]{3,2,1,0:T(4,128)(2,1)S(1)} copy(bf16[32,4,4,1024]{3,0,1,2:T(8,128)(2,1)S(1)} %bitcast.15) | data formatting | bytes 2097152 | tf_op jit(solution)/shard_map/transpose | solution.py:457
  42.9 1.1 %reshape.31 = bf16[512,1024]{1,0:T(8,128)(2,1)} reshape(bf16[32,4,4,1024]{3,2,1,0:T(4,128)(2,1)S(1)} %copy.8) | data formatting | bytes 2097152 | tf_op jit(solution)/shard_map/reshape | solution.py:457
Async XLA Ops:
  0.0 4.3 %copy-start = (bf16[1024,1024]{1,0:T(8,128)(2,1)S(1)}, bf16[1024,1024]{1,0:T(8,128)(2,1)}, u32[]{:S(2)}) copy-start(bf16[1024,1024]{1,0:T(8,128)(2,1)} %w_ref.1) | copy-start | bytes 6291460
where the time goes:
time: 44.2 us; the launch traced here: 44 us
  Pallas kernels  37.7 us (85%)
  local copies, waits for them, and re-layouts  6.23 us (14%)
    pallas_call x1, Pallas kernels, local(): pl.pallas_call(functools.partial(kernel, group), out_shape=jax.ShapeDtype...  37.7 us
    reshape x3, local copies, waits for them, and re-layouts, by_residue(): x = x.reshape(piece, RATIO, DILATION_TWO, group, dim)  4.31 us
    reshape x1, local copies, waits for them, and re-layouts, local(): return jnp.transpose(mixed, (2, 1, 0, 3)).reshape(tokens, columns)  1.11 us

commit v1 on v0

--- a/solution.py
+++ b/solution.py
@@ -17,6 +17,7 @@
 RATIO = DILATION_THREE // DILATION_TWO
 CHUNKS = DILATION_TWO
 ROWS_ONE = 16
+PARTS = 4
 ROWS_TWO = WINDOW_TWO // DILATION_THREE
 
 
@@ -50,10 +51,13 @@
 
 
 def kernel(
-    group, q_ref, k_ref, v_ref, w_ref, o_ref,
-    qb, kb, vb, acc, mx, sm, ob, ab, bias1, bias1f, bias2, bias2f, bias3,
-    in_send, in_recv, z_send, z_recv, zl_send, zl_recv, o_send, o_recv, d_send, d_recv,
+    group, q_hbm, k_hbm, v_hbm, w_hbm, *refs
 ):
+    o_refs = refs[:PARTS]
+    (
+    nat, raw, wide, q_ref, k_ref, v_ref, w_ref, qb, kb, vb, acc, mx, sm, ob, ab, bias1, bias1f, bias2, bias2f, bias3,
+    load, in_send, in_recv, z_send, z_recv, zl_send, zl_recv, o_send, o_recv, d_send, d_recv,
+    ) = refs[PARTS:]
     res, dim = DILATION_THREE, q_ref.shape[-1]
     piece = q_ref.shape[2]
     rows = group * piece
@@ -66,6 +70,12 @@
     partner = n_tp - 1 - tp
     scale = math.log2(math.e) / math.sqrt(dim)
 
+    loads = [
+        pltpu.make_async_copy(source, place, load.at[i])
+        for i, (source, place) in enumerate(
+            ((k_hbm, raw.at[0]), (v_hbm, raw.at[1]), (q_hbm, raw.at[2]), (w_hbm, w_ref))
+        )
+    ]
     barrier = pltpu.get_barrier_semaphore()
     for d in range(1, group):
         pl.semaphore_signal(
@@ -81,7 +91,8 @@
     def _():
         pl.semaphore_signal(barrier, inc=1, device_id={"sp": sp + group}, device_id_type=MESH)
 
-    pl.semaphore_wait(barrier, group + jnp.where(has_prev, 1, 0) + jnp.where(has_next, 1, 0))
+    for copy in loads:
+        copy.start()
 
     def span(start):
         return pl.ds(pl.multiple_of(start, piece), piece)
@@ -156,20 +167,19 @@
     whole = range(group // 2)
     split = range(group // 2, group)
 
-    @pl.when(has_next)
-    def _():
-        for which in (0, 1):
-            onward_rows(which, 0).start()
-
     near = [d for d in range(1, group) if d & (d - 1) == 0]
     far = [d for d in range(1, group) if d & (d - 1)]
-    for tensors_now in ((0, 1), (2,)):
-        for members in (near, far):
-            for which in tensors_now:
-                for d in members:
-                    exchange(which, d).start()
-
-    for source, buffer, offset in tensors:
+    pad = (res + 1) * group
+    for which, (source, buffer, offset) in enumerate(tensors):
+        loads[which].wait()
+        for i in range(piece):
+            tokens = raw[which, pl.ds(i * res, res)].astype(jnp.float32)
+            wide[which, pl.ds(i * pad, res * group), :] = tokens.reshape(res * group, dim)
+        for h in range(group):
+            for r in range(res):
+                store = r % DILATION_TWO * RATIO + r // DILATION_TWO
+                rows_of = wide[which, pl.ds(r * group + h, piece, stride=pad), :]
+                source[h, store] = rows_of.astype(source.dtype)
         buffer[:, span(offset + piece * mine), :] = source[mine]
 
     @pl.when(jnp.logical_not(has_prev))
@@ -207,14 +217,28 @@
         bias3.shape, lambda i: (i + rows, i), lambda i: (i, i), rows, WINDOW_THREE // DILATION_THREE, has_prev
     )
 
-    for k in range(1, group):
+    pl.semaphore_wait(barrier, group + jnp.where(has_prev, 1, 0) + jnp.where(has_next, 1, 0))
+
+    @pl.when(has_next)
+    def _():
         for which in (0, 1):
-            arrival(which, k).wait_recv()
-
-        @pl.when(has_next)
-        def _():
-            for which in (0, 1):
-                onward_rows(which, k).start()
+            onward_rows(which, 0).start()
+
+    for tensors_now in ((0, 1), (2,)):
+        for members in (near, far):
+            for which in tensors_now:
+                for d in members:
+                    exchange(which, d).start()
+
+    for members in (near, far):
+        for which in (0, 1):
+            for k in members:
+                arrival(which, k).wait_recv()
+
+            @pl.when(has_next)
+            def _():
+                for k in members:
+                    onward_rows(which, k).start()
 
     @pl.when(has_next)
     def _():
@@ -359,7 +383,10 @@
             swapped(s, d).wait_recv()
         attended = ab[part].reshape(RATIO * piece, -1)
         mixed = jnp.dot(attended, w_ref[...], preferred_element_type=jnp.float32)
-        o_ref[part] = mixed.astype(o_ref.dtype).reshape(RATIO, piece, -1)
+        for c in range(mixed.shape[1] // dim):
+            for j in range(RATIO):
+                at = pl.ds(s + DILATION_TWO * j, piece, stride=res + 1)
+                nat[c, at, :] = mixed[j * piece : (j + 1) * piece, c * dim : (c + 1) * dim]
 
     for s in range(CHUNKS):
         part = pl.ds(s * RATIO, RATIO)
@@ -382,11 +409,19 @@
         ab[part, :, lanes(head)] = ob[part, span(piece * mine), :]
         if s >= 2:
             hand_over(s - 2)
+    loads[3].wait()
     for s in range(CHUNKS - 2, CHUNKS):
         hand_over(s)
         project(s - 2)
     for s in range(CHUNKS - 2, CHUNKS):
         project(s)
+
+    per = piece // PARTS
+    for i in range(piece):
+        for c in range(nat.shape[0]):
+            o_refs[i // per][i % per * res : i % per * res + res, c * dim : (c + 1) * dim] = nat[
+                c, i * (res + 1) : i * (res + 1) + res, :
+            ].astype(jnp.bfloat16)
 
     for which in (0, 1, 2):
         for d in range(1, group):
@@ -417,19 +452,23 @@
     assert group & (group - 1) == 0 and piece > ROWS_ONE
     assert group * tokens == WINDOW_THREE and lax.axis_size("sp") % group == 0 and lax.axis_size("tp") == 2
 
-    def by_residue(x):
-        x = x.reshape(piece, RATIO, DILATION_TWO, group, dim)
-        return jnp.transpose(x, (3, 2, 1, 0, 4)).reshape(group, res, piece, dim)
-
     low, full = jnp.bfloat16, jnp.float32
     dma = pltpu.SemaphoreType.DMA
     vmem = pl.BlockSpec(memory_space=pltpu.VMEM)
+    hbm = pl.BlockSpec(memory_space=pltpu.HBM)
     mixed = pl.pallas_call(
         functools.partial(kernel, group),
-        out_shape=jax.ShapeDtypeStruct((res, piece, columns), low),
-        in_specs=[vmem] * 4,
-        out_specs=vmem,
+        out_shape=[jax.ShapeDtypeStruct((tokens // PARTS, columns), low)] * PARTS,
+        in_specs=[hbm] * 4,
+        out_specs=[vmem] * PARTS,
         scratch_shapes=[
+            pltpu.VMEM((columns // dim, piece * (res + 1), dim), full),
+            pltpu.VMEM((3, tokens, group, dim), low),
+            pltpu.VMEM((3, piece * (res + 1) * group, dim), full),
+            pltpu.VMEM((group, res, piece, dim), low),
+            pltpu.VMEM((group, res, piece, dim), low),
+            pltpu.VMEM((group, res, piece, dim), low),
+            pltpu.VMEM((features, columns), low),
             pltpu.VMEM((res, rows, dim), low),
             pltpu.VMEM((res, 2 * rows, dim), low),
             pltpu.VMEM((res, 2 * rows, dim), low),
@@ -443,6 +482,7 @@
             pltpu.VMEM((RATIO * ROWS_TWO, 2 * RATIO * ROWS_TWO), full),
             pltpu.VMEM((RATIO * ROWS_TWO, 2 * RATIO * ROWS_TWO), full),
             pltpu.VMEM((rows, 2 * rows), full),
+            dma((4,)),
             dma((3, group)), dma((3, group)),
             dma((2, group)), dma((2, group)),
             dma((2, group, CHUNKS)), dma((2, group, CHUNKS)),
@@ -450,11 +490,10 @@
             dma((CHUNKS, group)), dma((CHUNKS, group)),
         ],
         compiler_params=pltpu.CompilerParams(
-            collective_id=0, has_side_effects=True, vmem_limit_bytes=48 * 2**20
+            collective_id=0, has_side_effects=True, vmem_limit_bytes=55_000_000
         ),
-    )(by_residue(queries), by_residue(keys), by_residue(values), w_out)
-    mixed = mixed.reshape(DILATION_TWO, RATIO, piece, columns)
-    return jnp.transpose(mixed, (2, 1, 0, 3)).reshape(tokens, columns)
+    )(queries, keys, values, w_out)
+    return jnp.concatenate(mixed, axis=0)
 
 
 def solution(mesh):

time: 44.2 us -> 39.8 us (0.900)
  local copies, waits for them, and re-layouts: 6.23 us -> 0 us
  other arithmetic: 0 us -> 1.04 us
  Pallas kernels: 37.7 us -> 38.6 us
    reshape x4 -> x0, local copies, waits for them, and re-layouts: 5.41 us -> none  [the longest x3 4.31 us: by_residue(): x = x.reshape(piece, RATIO, DILATION_TWO, group, dim)]
    concatenate x0 -> x1, other arithmetic: none -> 1.04 us  [local(): return jnp.concatenate(mixed, axis=0)]
    pallas_call x1, Pallas kernels: 37.7 us -> 38.6 us  [local(): pl.pallas_call(functools.partial(kernel, group), out_shape=[jax.ShapeDtyp...]
    transpose x1 -> x0, local copies, waits for them, and re-layouts: 0.81 us -> none  [local(): return jnp.transpose(mixed, (2, 1, 0, 3)).reshape(tokens, columns)]
where the time goes in v1:
time: 39.8 us; the launch traced here: 39.7 us
  Pallas kernels  38.6 us (97%)
  other arithmetic  1.04 us (3%)
    pallas_call x1, Pallas kernels, local(): pl.pallas_call(functools.partial(kernel, group), out_shape=[jax.ShapeDtyp...  38.6 us
    concatenate x1, other arithmetic, local(): return jnp.concatenate(mixed, axis=0)  1.04 us

profile of v1, /device:TPU:0, one launch (start us, length us, event | category | flops | bytes accessed | tf_op | source)
XLA Modules:
  0.0 39.7 jit_solution(8946421115237333960)
XLA Ops:
  0.0 38.6 %shard_map.46 = (bf16[128,1024]{1,0:T(8,128)(2,1)S(1)}, bf16[128,1024]{1,0:T(8,128)(2,1)S(1)}, bf16[128,1024]{1,0:T(8,128)(2,1)S(1)}, bf16[128,1024]{1,0:T(8,128)(2,1)S(1)}) custom-call(bf16[512,4,128]{2,1,0:T(4,128)(2,1)} %q_hbm.1, bf16[512,4,128]{2,1,0:T(4,128)(2,1)} %k_hbm.1, bf16[512,4,128]{2,1,0:T(4,128)(2,1)} %v_hbm.1, bf16[1024,1024]{1,0:T(8,128)(2,1)} %w_hbm.1), custom_call_target="tpu_custom_call" | custom-call | tf_op jit(solution)/shard_map/pallas_call | solution.py:459
  38.6 1.0 %pad_maximum_fusion = bf16[512,1024]{1,0:T(8,128)(2,1)} fusion(bf16[128,1024]{1,0:T(8,128)(2,1)S(1)} %get-tuple-element.12, bf16[128,1024]{1,0:T(8,128)(2,1)S(1)} %get-tuple-element.11, bf16[128,1024]{1,0:T(8,128)(2,1)S(1)} %get-tuple-element.10, bf16[128,1024]{1,0:T(8,128)(2,1)S(1)} %get-tuple-element.9), kind=kLoop, calls=%fused_computation | loop fusion | flops 4194304 | bytes 2097152 | tf_op jit(solution)/shard_map/concatenate | solution.py:496

commit v2 on v1

v2 whole, which is shorter than its diff:
```python
import functools
import math

import jax
import jax.numpy as jnp
from jax import lax
from jax.experimental import pallas as pl
from jax.experimental.pallas import tpu as pltpu
from jax.sharding import PartitionSpec as P

W1 = 128
WINDOW_TWO = 512
DILATION_TWO = 4
WINDOW_THREE = 2048
DILATION_THREE = 16
MESH = pl.DeviceIdType.MESH
RATIO = DILATION_THREE // DILATION_TWO
CHUNKS = DILATION_TWO
ROWS_ONE = 16
PARTS = 4
UNITS = ((0, 4), (4, 4), (8, 4), (12, 2), (14, 2))
ROWS_TWO = WINDOW_TWO // DILATION_THREE


def attend(blocks, scale):
    scores = [
        lax.dot_general(q, k, (((1,), (1,)), ((), ())), preferred_element_type=jnp.float32)
        for q, k, _, _ in blocks
    ]
    scores = [x * scale + bias for x, (_, _, _, bias) in zip(scores, blocks)]
    tops = [jnp.max(x, axis=-1, keepdims=True) for x in scores]
    numerators = [jnp.exp2(x - top) for x, top in zip(scores, tops)]
    sums = [
        jnp.dot(
            x.astype(v.dtype), jnp.concatenate([v, jnp.ones_like(v)], axis=1), preferred_element_type=jnp.float32
        )
        for x, (_, _, v, _) in zip(numerators, blocks)
    ]
    dim = blocks[0][2].shape[-1]
    return [(x[:, :dim], jnp.broadcast_to(top, x[:, :dim].shape), x[:, dim:]) for x, top in zip(sums, tops)]


def bias_of(shape, place_q, place_k, first_own, window, has_prev):
    query_place, _ = place_q(lax.broadcasted_iota(jnp.int32, shape, 0))
    key_place, key_row = place_k(lax.broadcasted_iota(jnp.int32, shape, 1))
    distance = query_place - key_place
    allowed = (distance >= 0) & (distance <= window)
    general = jnp.where(allowed, 0.0, -jnp.inf).astype(jnp.float32)
    gate = jnp.where(has_prev, 0, first_own)
    first = jnp.where(allowed & (key_row >= gate), 0.0, -jnp.inf).astype(jnp.float32)
    return general, first


def kernel(
    group, q_hbm, k_hbm, v_hbm, w_hbm, *refs
):
    o_refs = refs[:PARTS]
    (
    nat, raw, wide, q_ref, k_ref, v_ref, w_ref, qb, kb, vb, acc, mx, sm, ob, ab, bias1, bias2, bias2f, bias3,
    load, in_send, in_recv, q_send, q_recv, z_send, z_recv, zb_send, zb_recv, zc_send, zc_recv, o_send, o_recv, d_send, d_recv,
    ) = refs[PARTS:]
    res, dim = DILATION_THREE, q_ref.shape[-1]
    piece = q_ref.shape[2]
    rows = group * piece
    sp, tp = lax.axis_index("sp"), lax.axis_index("tp")
    n_sp, n_tp = lax.axis_size("sp"), lax.axis_size("tp")
    mine = lax.rem(sp, group)
    base = sp - mine
    has_prev = sp >= group
    has_next = sp + group < n_sp
    partner = n_tp - 1 - tp
    scale = math.log2(math.e) / math.sqrt(dim)

    loads = [
        pltpu.make_async_copy(source, place, load.at[i])
        for i, (source, place) in enumerate(
            ((k_hbm, raw.at[0]), (v_hbm, raw.at[1]), (q_hbm, raw.at[2]), (w_hbm, w_ref))
        )
    ]
    barrier = pltpu.get_barrier_semaphore()
    for d in range(1, group):
        pl.semaphore_signal(
            barrier, inc=1, device_id={"sp": base + lax.rem(mine + d, group)}, device_id_type=MESH
        )
    pl.semaphore_signal(barrier, inc=1, device_id={"tp": partner}, device_id_type=MESH)

    @pl.when(has_prev)
    def _():
        pl.semaphore_signal(barrier, inc=1, device_id={"sp": sp - group}, device_id_type=MESH)

    @pl.when(has_next)
    def _():
        pl.semaphore_signal(barrier, inc=1, device_id={"sp": sp + group}, device_id_type=MESH)

    for copy in loads:
        copy.start()

    def span(start):
        return pl.ds(pl.multiple_of(start, piece), piece)

    tensors = ((k_ref, kb, rows), (v_ref, vb, rows), (q_ref, qb, 0))

    def member(d):
        other, bit = mine, 1
        while bit <= d:
            if d & bit:
                other = other + bit * (1 - 2 * lax.rem(mine // bit, 2))
            bit *= 2
        return other

    def exchange(which, d, s=None):
        source, buffer, offset = tensors[which]
        other = member(d)
        part = slice(None) if s is None else pl.ds(s * RATIO, RATIO)
        return pltpu.make_async_remote_copy(
            src_ref=source.at[other, part],
            dst_ref=buffer.at[part, span(offset + piece * mine), :],
            send_sem=in_send.at[which, d] if s is None else q_send.at[s],
            recv_sem=in_recv.at[which, d] if s is None else q_recv.at[s],
            device_id={"sp": base + other},
            device_id_type=MESH,
        )

    def arrival(which, d, s=None):
        source, buffer, offset = tensors[which]
        part = slice(None) if s is None else pl.ds(s * RATIO, RATIO)
        return pltpu.make_async_remote_copy(
            src_ref=source.at[0, part],
            dst_ref=buffer.at[part, span(offset + piece * member(d)), :],
            send_sem=in_send.at[which, d] if s is None else q_send.at[s],
            recv_sem=in_recv.at[which, d] if s is None else q_recv.at[s],
            device_id={"sp": sp},
            device_id_type=MESH,
        )

    low = piece - ROWS_ONE

    last = group - 1
    swapped_roles = member(2) == last
    early = jnp.where(swapped_roles, member(2), member(3))
    late = jnp.where(swapped_roles, member(3), member(2))

    def onward(which, src, dst, send, recv):
        return pltpu.make_async_remote_copy(
            src_ref=src,
            dst_ref=dst,
            send_sem=send,
            recv_sem=recv,
            device_id={"sp": sp + group},
            device_id_type=MESH,
        )

    def onward_rows(which, k):
        source, buffer, _ = tensors[which]
        start = piece * (mine, member(1), early)[k]
        if k == 0:
            src, dst = source.at[mine], buffer.at[:, span(start), :]
        elif k == 1:
            src, dst = buffer.at[:, span(rows + start), :], buffer.at[:, span(start), :]
        else:
            ends = [pl.ds(pl.multiple_of(x + start + low, ROWS_ONE), ROWS_ONE) for x in (rows, 0)]
            src, dst = (buffer.at[:, x, :] for x in ends)
        return onward(which, src, dst, z_send.at[which, k], z_recv.at[which, k])

    def onward_early(which, u):
        _, buffer, _ = tensors[which]
        ends = [pl.ds(pl.multiple_of(x + piece * early, ROWS_ONE), low) for x in (rows, 0)]
        src, dst = (buffer.at[pl.ds(*UNITS[u]), x, :] for x in ends)
        return onward(which, src, dst, zc_send.at[which, u], zc_recv.at[which, u])

    def onward_late(which, u):
        _, buffer, _ = tensors[which]
        src, dst = (buffer.at[pl.ds(*UNITS[u]), span(x + piece * late), :] for x in (rows, 0))
        return onward(which, src, dst, zb_send.at[which, u], zb_recv.at[which, u])

    near = [d for d in range(1, group) if d & (d - 1) == 0]
    far = [d for d in range(1, group) if d & (d - 1)]
    pad = (res + 1) * group
    for which, (source, buffer, offset) in enumerate(tensors):
        loads[which].wait()
        for i in range(piece):
            tokens = raw[which, pl.ds(i * res, res)].astype(jnp.float32)
            wide[which, pl.ds(i * pad, res * group), :] = tokens.reshape(res * group, dim)
        for h in range(group):
            for r in range(res):
                store = r % DILATION_TWO * RATIO + r // DILATION_TWO
                rows_of = wide[which, pl.ds(r * group + h, piece, stride=pad), :]
                source[h, store] = rows_of.astype(source.dtype)
        buffer[:, span(offset + piece * mine), :] = source[mine]

    @pl.when(jnp.logical_not(has_prev))
    def _():
        kb[:, :rows, :] = jnp.zeros((res, rows, dim), kb.dtype)
        vb[:, :rows, :] = jnp.zeros((res, rows, dim), vb.dtype)

    def place_one(per):
        def place(i):
            store, row = i // per, i % per
            residue = (store % RATIO) * DILATION_TWO + store // RATIO
            return row * res + residue, row
        return place

    def place_two(per):
        def place(i):
            j, row = i // per, i % per
            return row * RATIO + j, row
        return place

    def shifted(place, by):
        def moved(i):
            at, row = place(i)
            return at + by, row
        return moved

    bias1[0], bias1[1] = bias_of(
        bias1.shape[1:], shifted(place_one(ROWS_ONE), ROWS_ONE * res), place_one(2 * ROWS_ONE), ROWS_ONE, W1, has_prev
    )
    bias2[...], bias2f[...] = bias_of(
        bias2.shape, shifted(place_two(ROWS_TWO), ROWS_TWO * RATIO), place_two(2 * ROWS_TWO), ROWS_TWO,
        WINDOW_TWO // DILATION_TWO, has_prev,
    )
    _, bias3[...] = bias_of(
        bias3.shape, lambda i: (i + rows, i), lambda i: (i, i), rows, WINDOW_THREE // DILATION_THREE, has_prev
    )

    pl.semaphore_wait(barrier, group + jnp.where(has_prev, 1, 0) + jnp.where(has_next, 1, 0))

    @pl.when(has_next)
    def _():
        for which in (0, 1):
            onward_rows(which, 0).start()

    for members in (near, far):
        for which in (0, 1):
            for d in members:
                exchange(which, d).start()

    def pass_on(*copies):
        @pl.when(has_next)
        def _():
            for copy in copies:
                copy.start()

    def one(b, first=0, s=None):
        own = pl.ds(pl.multiple_of(b * ROWS_ONE, ROWS_ONE), ROWS_ONE)
        near_rows = pl.ds(pl.multiple_of(rows + (b - 1) * ROWS_ONE, ROWS_ONE), 2 * ROWS_ONE)
        start, count = (0, res) if s is None else (s * RATIO, RATIO)
        part = pl.ds(start, count)

        def keep(found):
            for ref, value in zip((acc, mx, sm), found):
                ref[part, own, :] = value.reshape(count, ROWS_ONE, dim)

        block = (
            qb[part, own, :].reshape(-1, dim),
            kb[:, near_rows, :].reshape(-1, dim),
            vb[:, near_rows, :].reshape(-1, dim),
            bias1[first, pl.ds(start * ROWS_ONE, count * ROWS_ONE), :],
        )
        return block, keep

    def merge(at, weighted, top, total):
        old_top = mx[at].reshape(-1, dim)
        new_top = jnp.maximum(old_top, top)
        old_part, part = jnp.exp2(old_top - new_top), jnp.exp2(top - new_top)
        return (
            acc[at].reshape(-1, dim) * old_part + weighted * part,
            new_top,
            sm[at].reshape(-1, dim) * old_part + total * part,
        )

    def two(s, b, bias=None):
        bias = bias2 if bias is None else bias
        part = pl.ds(s * RATIO, RATIO)
        own = pl.ds(pl.multiple_of(b * ROWS_TWO, ROWS_TWO), ROWS_TWO)
        near_rows = pl.ds(pl.multiple_of(rows + (b - 1) * ROWS_TWO, ROWS_TWO), 2 * ROWS_TWO)

        def keep(found):
            merged = merge((part, own, slice(None)), *found)
            for ref, value in zip((acc, mx, sm), merged):
                ref[part, own, :] = value.reshape(RATIO, ROWS_TWO, dim)

        block = tuple(x[part, at, :].reshape(-1, dim) for x, at in ((qb, own), (kb, near_rows), (vb, near_rows)))
        return block + (bias[...],), keep

    def three(x):
        def keep(found):
            weighted, _, total = merge((x,), *found)
            ob[x] = (weighted / total).astype(ob.dtype)

        return (qb[x], kb[x], vb[x], bias3[...]), keep

    def run(*groups):
        parts = [item for items, _ in groups for item in items]
        found = iter(attend([block for block, _ in parts], scale))
        for items, after in groups:
            for _, keep in items:
                keep(next(found))
            after()

    def nothing():
        pass

    def some(items, count):
        return [items[i : i + count] for i in range(0, len(items), count)]

    steps = piece // ROWS_ONE
    soon = mine + 1 - mine % 2
    later = (group // 2, group - soon)
    near_far = 2 + jnp.where(mine == 1, 1, 0)
    edge = jnp.where(mine == last, 1, 0)
    for d in near:
        arrival(0, d).wait_recv()
    pass_on(onward_rows(0, 1))
    for d in near:
        arrival(1, d).wait_recv()
    pass_on(onward_rows(1, 1))
    for d in far:
        arrival(0, d).wait_recv()
    for d in near:
        exchange(2, d).start()
    for s in range(CHUNKS):
        for d in far:
            exchange(2, d, s).start()
    pass_on(onward_rows(0, 2), onward_late(0, 0), onward_early(0, 0))
    for d in far:
        arrival(1, d).wait_recv()
    pass_on(
        onward_rows(1, 2), onward_late(1, 0), onward_early(1, 0),
        *[f(x, u) for u in (1, 2) for f in (onward_late, onward_early) for x in (0, 1)],
        *[f(x, u) for f in (onward_early, onward_late) for u in (3, 4) for x in (0, 1)],
    )
    def inners(d, s=None):
        return [one(member(d) * steps + inner, 0, s) for inner in range(1, steps)]

    run((inners(0), nothing))
    for d in near:
        arrival(2, d).wait_recv()
    for d, b in zip(near, (soon, near_far)):
        run((inners(d) + [one(b * steps)], nothing))
    run(([two(s, soon) for s in range(CHUNKS)], nothing))

    @pl.when(has_prev)
    def _():
        for k in range(3):
            for which in (0, 1):
                onward_rows(which, k).wait_recv()

    def sooner(s):
        if s == CHUNKS:
            return []
        for d in far:
            arrival(2, d, s).wait_recv()
        found = []
        for d in far:
            found += inners(d, s) + [one(member(d) * steps, jnp.where(member(d) == 0, 1, 0), s)]
        return found + [two(s, b) for b in later]

    run(([one(edge * steps, 1 - edge)] + sooner(0), nothing))

    head = tp * group + mine

    def lanes(index):
        return pl.ds(pl.multiple_of(index * dim, dim), dim)

    def give(u, d):
        part = pl.ds(*UNITS[u])
        other = member(d)
        return pltpu.make_async_remote_copy(
            src_ref=ob.at[part, span(piece * other), :],
            dst_ref=ab.at[part, :, lanes(head)],
            send_sem=o_send.at[u, d],
            recv_sem=o_recv.at[u, d],
            device_id={"sp": base + other},
            device_id_type=MESH,
        )

    def taken(u, d):
        part = pl.ds(*UNITS[u])
        return pltpu.make_async_remote_copy(
            src_ref=ob.at[part, span(0), :],
            dst_ref=ab.at[part, :, lanes(tp * group + member(d))],
            send_sem=o_send.at[u, d],
            recv_sem=o_recv.at[u, d],
            device_id={"sp": sp},
            device_id_type=MESH,
        )

    def swap(u, d):
        part = pl.ds(*UNITS[u])
        slot = ab.at[part, :, lanes(tp * group + member(d))]
        return pltpu.make_async_remote_copy(
            src_ref=ob.at[part, span(piece * mine), :] if d == 0 else slot,
            dst_ref=slot,
            send_sem=d_send.at[u, d],
            recv_sem=d_recv.at[u, d],
            device_id={"tp": partner},
            device_id_type=MESH,
        )

    def swapped(u, d):
        part = pl.ds(*UNITS[u])
        return pltpu.make_async_remote_copy(
            src_ref=ob.at[part, span(0), :],
            dst_ref=ab.at[part, :, lanes(partner * group + member(d))],
            send_sem=d_send.at[u, d],
            recv_sem=d_recv.at[u, d],
            device_id={"tp": partner},
            device_id_type=MESH,
        )

    def hand_over(u):
        for d in range(1, group):
            taken(u, d).wait_recv()
            swap(u, d).start()

    def project(u):
        start, count = UNITS[u]
        for d in range(group):
            swapped(u, d).wait_recv()
        attended = ab[pl.ds(start, count)].reshape(count * piece, -1)
        mixed = jnp.dot(attended, w_ref[...], preferred_element_type=jnp.float32)
        for c in range(mixed.shape[1] // dim):
            for j in range(count):
                residue = (start + j) // RATIO + (start + j) % RATIO * DILATION_TWO
                at = pl.ds(residue, piece, stride=res + 1)
                nat[c, at, :] = mixed[j * piece : (j + 1) * piece, c * dim : (c + 1) * dim]

    def from_prev(*copies):
        @pl.when(has_prev)
        def _():
            for copy in copies:
                copy.wait_recv()

    def hand_out(u):
        def now():
            part = pl.ds(*UNITS[u])
            for d in far + near:
                give(u, d).start()
            swap(u, 0).start()
            ab[part, :, lanes(head)] = ob[part, span(piece * mine), :]

        return now

    def threes(u):
        start, count = UNITS[u]
        return [three(x) for x in range(start, start + count)]

    for s in range(CHUNKS):
        units = [u for u, (start, _) in enumerate(UNITS) if start // RATIO == s]
        from_prev(*[onward_early(x, u) for u in units for x in (0, 1)])
        from_prev(*[onward_late(x, units[0]) for x in (0, 1)])
        run(
            ([two(s, 0, bias2f)] + threes(units[0]), hand_out(units[0])),
            (sooner(s + 1), nothing),
        )
        for u in units[1:]:
            from_prev(*[onward_late(x, u) for x in (0, 1)])
            run((threes(u), hand_out(u)))
        if s == 2:
            hand_over(0)
    loads[3].wait()
    for u in range(1, len(UNITS)):
        hand_over(u)
        project(u - 1)
    project(len(UNITS) - 1)

    per = piece // PARTS
    for i in range(piece):
        for c in range(nat.shape[0]):
            o_refs[i // per][i % per * res : i % per * res + res, c * dim : (c + 1) * dim] = nat[
                c, i * (res + 1) : i * (res + 1) + res, :
            ].astype(jnp.bfloat16)

    for which in (0, 1):
        for d in range(1, group):
            exchange(which, d).wait_send()
    for d in near:
        exchange(2, d).wait_send()
    for d in far:
        for s in range(CHUNKS):
            exchange(2, d, s).wait_send()

    @pl.when(has_next)
    def _():
        for which in (0, 1):
            for k in range(3):
                onward_rows(which, k).wait_send()
            for u in range(len(UNITS)):
                onward_early(which, u).wait_send()
                onward_late(which, u).wait_send()

    for u in range(len(UNITS)):
        for d in range(1, group):
            give(u, d).wait_send()
        for d in range(group):
            swap(u, d).wait_send()


def local(queries, keys, values, w_out):
    tokens, group, dim = queries.shape
    features, columns = w_out.shape
    res = DILATION_THREE
    piece = tokens // res
    rows = group * piece
    assert group == 4 and piece > ROWS_ONE
    assert group * tokens == WINDOW_THREE and lax.axis_size("sp") % group == 0 and lax.axis_size("tp") == 2

    low, full = jnp.bfloat16, jnp.float32
    dma = pltpu.SemaphoreType.DMA
    vmem = pl.BlockSpec(memory_space=pltpu.VMEM)
    hbm = pl.BlockSpec(memory_space=pltpu.HBM)
    mixed = pl.pallas_call(
        functools.partial(kernel, group),
        out_shape=[jax.ShapeDtypeStruct((tokens // PARTS, columns), low)] * PARTS,
        in_specs=[hbm] * 4,
        out_specs=[vmem] * PARTS,
        scratch_shapes=[
            pltpu.VMEM((columns // dim, piece * (res + 1), dim), full),
            pltpu.VMEM((3, tokens, group, dim), low),
            pltpu.VMEM((3, piece * (res + 1) * group, dim), full),
            pltpu.VMEM((group, res, piece, dim), low),
            pltpu.VMEM((group, res, piece, dim), low),
            pltpu.VMEM((group, res, piece, dim), low),
            pltpu.VMEM((features, columns), low),
            pltpu.VMEM((res, rows, dim), low),
            pltpu.VMEM((res, 2 * rows, dim), low),
            pltpu.VMEM((res, 2 * rows, dim), low),
            pltpu.VMEM((res, rows, dim), full),
            pltpu.VMEM((res, rows, dim), full),
            pltpu.VMEM((res, rows, dim), full),
            pltpu.VMEM((res, rows, dim), low),
            pltpu.VMEM((res, piece, features), low),
            pltpu.VMEM((2, res * ROWS_ONE, 2 * res * ROWS_ONE), full),
            pltpu.VMEM((RATIO * ROWS_TWO, 2 * RATIO * ROWS_TWO), full),
            pltpu.VMEM((RATIO * ROWS_TWO, 2 * RATIO * ROWS_TWO), full),
            pltpu.VMEM((rows, 2 * rows), full),
            dma((4,)),
            dma((3, group)), dma((3, group)),
            dma((CHUNKS,)), dma((CHUNKS,)),
            dma((2, 3)), dma((2, 3)),
            dma((2, len(UNITS))), dma((2, len(UNITS))),
            dma((2, len(UNITS))), dma((2, len(UNITS))),
            dma((len(UNITS), group)), dma((len(UNITS), group)),
            dma((len(UNITS), group)), dma((len(UNITS), group)),
        ],
        compiler_params=pltpu.CompilerParams(
            collective_id=0, has_side_effects=True, vmem_limit_bytes=55_000_000
        ),
    )(queries, keys, values, w_out)
    return jnp.concatenate(mixed, axis=0)


def solution(mesh):
    in_specs = (P("sp", "tp", None), P("sp", "tp", None), P("sp", "tp", None), P(None, "tp"))
    out_specs = P("sp", "tp")
    return jax.shard_map(local, mesh=mesh, in_specs=in_specs, out_specs=out_specs, check_vma=False)
```

time: 39.8 us -> 36.5 us (0.917)
  Pallas kernels: 38.6 us -> 35.1 us
    pallas_call x1, Pallas kernels: 38.6 us -> 35.1 us  [local(): pl.pallas_call(functools.partial(kernel, group), out_shape=[jax.ShapeDtyp...]
where the time goes in v2:
time: 36.5 us; the launch traced here: 36.1 us
  Pallas kernels  35.1 us (96%)
  other arithmetic  1.04 us (3%)
    pallas_call x1, Pallas kernels, local(): pl.pallas_call(functools.partial(kernel, group), out_shape=[jax.ShapeDtyp...  35.1 us
    concatenate x1, other arithmetic, local(): return jnp.concatenate(mixed, axis=0)  1.04 us

profile of v2, /device:TPU:0, one launch (start us, length us, event | category | flops | bytes accessed | tf_op | source)
XLA Modules:
  0.0 36.1 jit_solution(3342060734455519379)
XLA Ops:
  0.0 35.1 %shard_map.46 = (bf16[128,1024]{1,0:T(8,128)(2,1)S(1)}, bf16[128,1024]{1,0:T(8,128)(2,1)S(1)}, bf16[128,1024]{1,0:T(8,128)(2,1)S(1)}, bf16[128,1024]{1,0:T(8,128)(2,1)S(1)}) custom-call(bf16[512,4,128]{2,1,0:T(4,128)(2,1)} %q_hbm.1, bf16[512,4,128]{2,1,0:T(4,128)(2,1)} %k_hbm.1, bf16[512,4,128]{2,1,0:T(4,128)(2,1)} %v_hbm.1, bf16[1024,1024]{1,0:T(8,128)(2,1)} %w_hbm.1), custom_call_target="tpu_custom_call" | custom-call | tf_op jit(solution)/shard_map/pallas_call | solution.py:513
  35.1 1.0 %pad_maximum_fusion = bf16[512,1024]{1,0:T(8,128)(2,1)} fusion(bf16[128,1024]{1,0:T(8,128)(2,1)S(1)} %get-tuple-element.12, bf16[128,1024]{1,0:T(8,128)(2,1)S(1)} %get-tuple-element.11, bf16[128,1024]{1,0:T(8,128)(2,1)S(1)} %get-tuple-element.10, bf16[128,1024]{1,0:T(8,128)(2,1)S(1)} %get-tuple-element.9), kind=kLoop, calls=%fused_computation | loop fusion | flops 4194304 | bytes 2097152 | tf_op jit(solution)/shard_map/concatenate | solution.py:551

commit v3 on v2

--- a/solution.py
+++ b/solution.py
@@ -17,7 +17,8 @@
 RATIO = DILATION_THREE // DILATION_TWO
 CHUNKS = DILATION_TWO
 ROWS_ONE = 16
-PARTS = 4
+PARTS = 2
+QUERY_PARTS = ((0, 1), (1, 3))
 UNITS = ((0, 4), (4, 4), (8, 4), (12, 2), (14, 2))
 ROWS_TWO = WINDOW_TWO // DILATION_THREE
 
@@ -30,14 +31,15 @@
     scores = [x * scale + bias for x, (_, _, _, bias) in zip(scores, blocks)]
     tops = [jnp.max(x, axis=-1, keepdims=True) for x in scores]
     numerators = [jnp.exp2(x - top) for x, top in zip(scores, tops)]
-    sums = [
-        jnp.dot(
-            x.astype(v.dtype), jnp.concatenate([v, jnp.ones_like(v)], axis=1), preferred_element_type=jnp.float32
-        )
+    sums = [jnp.sum(x, axis=-1, keepdims=True) for x in numerators]
+    weighted = [
+        jnp.dot(x.astype(v.dtype), v, preferred_element_type=jnp.float32)
         for x, (_, _, v, _) in zip(numerators, blocks)
     ]
-    dim = blocks[0][2].shape[-1]
-    return [(x[:, :dim], jnp.broadcast_to(top, x[:, :dim].shape), x[:, dim:]) for x, top in zip(sums, tops)]
+    return [
+        (x, jnp.broadcast_to(top, x.shape), jnp.broadcast_to(total, x.shape))
+        for x, top, total in zip(weighted, tops, sums)
+    ]
 
 
 def bias_of(shape, place_q, place_k, first_own, window, has_prev):
@@ -111,7 +113,7 @@
     def exchange(which, d, s=None):
         source, buffer, offset = tensors[which]
         other = member(d)
-        part = slice(None) if s is None else pl.ds(s * RATIO, RATIO)
+        part = slice(None) if s is None else pl.ds(*(x * RATIO for x in QUERY_PARTS[s]))
         return pltpu.make_async_remote_copy(
             src_ref=source.at[other, part],
             dst_ref=buffer.at[part, span(offset + piece * mine), :],
@@ -123,7 +125,7 @@
 
     def arrival(which, d, s=None):
         source, buffer, offset = tensors[which]
-        part = slice(None) if s is None else pl.ds(s * RATIO, RATIO)
+        part = slice(None) if s is None else pl.ds(*(x * RATIO for x in QUERY_PARTS[s]))
         return pltpu.make_async_remote_copy(
             src_ref=source.at[0, part],
             dst_ref=buffer.at[part, span(offset + piece * member(d)), :],
@@ -244,7 +246,7 @@
     def one(b, first=0, s=None):
         own = pl.ds(pl.multiple_of(b * ROWS_ONE, ROWS_ONE), ROWS_ONE)
         near_rows = pl.ds(pl.multiple_of(rows + (b - 1) * ROWS_ONE, ROWS_ONE), 2 * ROWS_ONE)
-        start, count = (0, res) if s is None else (s * RATIO, RATIO)
+        start, count = (0, res) if s is None else (x * RATIO for x in QUERY_PARTS[s])
         part = pl.ds(start, count)
 
         def keep(found):
@@ -319,7 +321,7 @@
         arrival(0, d).wait_recv()
     for d in near:
         exchange(2, d).start()
-    for s in range(CHUNKS):
+    for s in range(len(QUERY_PARTS)):
         for d in far:
             exchange(2, d, s).start()
     pass_on(onward_rows(0, 2), onward_late(0, 0), onward_early(0, 0))
@@ -349,14 +351,13 @@
     def sooner(s):
         if s == CHUNKS:
             return []
-        for d in far:
-            arrival(2, d, s).wait_recv()
         found = []
-        for d in far:
-            found += inners(d, s) + [one(member(d) * steps, jnp.where(member(d) == 0, 1, 0), s)]
+        for i, (first, _) in enumerate(QUERY_PARTS):
+            for d in far if first == s else ():
+                arrival(2, d, i).wait_recv()
+                found += inners(d, i) + [one(member(d) * steps, jnp.where(member(d) == 0, 1, 0), i)]
         return found + [two(s, b) for b in later]
 
-    run(([one(edge * steps, 1 - edge)] + sooner(0), nothing))
 
     head = tp * group + mine
 
@@ -450,10 +451,8 @@
         units = [u for u, (start, _) in enumerate(UNITS) if start // RATIO == s]
         from_prev(*[onward_early(x, u) for u in units for x in (0, 1)])
         from_prev(*[onward_late(x, units[0]) for x in (0, 1)])
-        run(
-            ([two(s, 0, bias2f)] + threes(units[0]), hand_out(units[0])),
-            (sooner(s + 1), nothing),
-        )
+        edges = [one(edge * steps, 1 - edge)] if s == 0 else []
+        run((edges + sooner(s), nothing), ([two(s, 0, bias2f)] + threes(units[0]), hand_out(units[0])))
         for u in units[1:]:
             from_prev(*[onward_late(x, u) for x in (0, 1)])
             run((threes(u), hand_out(u)))
@@ -478,7 +477,7 @@
     for d in near:
         exchange(2, d).wait_send()
     for d in far:
-        for s in range(CHUNKS):
+        for s in range(len(QUERY_PARTS)):
             exchange(2, d, s).wait_send()
 
     @pl.when(has_next)
@@ -537,7 +536,7 @@
             pltpu.VMEM((rows, 2 * rows), full),
             dma((4,)),
             dma((3, group)), dma((3, group)),
-            dma((CHUNKS,)), dma((CHUNKS,)),
+            dma((len(QUERY_PARTS),)), dma((len(QUERY_PARTS),)),
             dma((2, 3)), dma((2, 3)),
             dma((2, len(UNITS))), dma((2, len(UNITS))),
             dma((2, len(UNITS))), dma((2, len(UNITS))),

time: 36.5 us -> 35.9 us (0.984)
  Pallas kernels: 35.1 us -> 34.4 us
    pallas_call x1, Pallas kernels: 35.1 us -> 34.4 us  [local(): pl.pallas_call(functools.partial(kernel, group), out_shape=[jax.ShapeDtyp...]
where the time goes in v3:
time: 35.9 us; the launch traced here: 35.5 us
  Pallas kernels  34.4 us (96%)
  other arithmetic  1.04 us (3%)
    pallas_call x1, Pallas kernels, local(): pl.pallas_call(functools.partial(kernel, group), out_shape=[jax.ShapeDtyp...  34.4 us
    concatenate x1, other arithmetic, local(): return jnp.concatenate(mixed, axis=0)  1.04 us

profile of v3, /device:TPU:0, one launch (start us, length us, event | category | flops | bytes accessed | tf_op | source)
XLA Modules:
  0.0 35.5 jit_solution(541609207169061627)
XLA Ops:
  0.0 34.4 %shard_map.46 = (bf16[256,1024]{1,0:T(8,128)(2,1)S(1)}, bf16[256,1024]{1,0:T(8,128)(2,1)S(1)}) custom-call(bf16[512,4,128]{2,1,0:T(4,128)(2,1)} %q_hbm.1, bf16[512,4,128]{2,1,0:T(4,128)(2,1)} %k_hbm.1, bf16[512,4,128]{2,1,0:T(4,128)(2,1)} %v_hbm.1, bf16[1024,1024]{1,0:T(8,128)(2,1)} %w_hbm.1), custom_call_target="tpu_custom_call" | custom-call | tf_op jit(solution)/shard_map/pallas_call | solution.py:512
  34.4 1.0 %pad_maximum_fusion = bf16[512,1024]{1,0:T(8,128)(2,1)} fusion(bf16[256,1024]{1,0:T(8,128)(2,1)S(1)} %get-tuple-element.8, bf16[256,1024]{1,0:T(8,128)(2,1)S(1)} %get-tuple-element.7), kind=kLoop, calls=%fused_computation | loop fusion | flops 2097152 | bytes 2097152 | tf_op jit(solution)/shard_map/concatenate | solution.py:550

commit v4 on v3

--- a/solution.py
+++ b/solution.py
@@ -28,7 +28,7 @@
         lax.dot_general(q, k, (((1,), (1,)), ((), ())), preferred_element_type=jnp.float32)
         for q, k, _, _ in blocks
     ]
-    scores = [x * scale + bias for x, (_, _, _, bias) in zip(scores, blocks)]
+    scores = [bias(x * scale) if callable(bias) else x * scale + bias for x, (_, _, _, bias) in zip(scores, blocks)]
     tops = [jnp.max(x, axis=-1, keepdims=True) for x in scores]
     numerators = [jnp.exp2(x - top) for x, top in zip(scores, tops)]
     sums = [jnp.sum(x, axis=-1, keepdims=True) for x in numerators]
@@ -58,7 +58,7 @@
 ):
     o_refs = refs[:PARTS]
     (
-    nat, raw, wide, q_ref, k_ref, v_ref, w_ref, qb, kb, vb, acc, mx, sm, ob, ab, bias1, bias2, bias2f, bias3,
+    nat, raw, wide, q_ref, k_ref, v_ref, w_ref, qb, kb, vb, acc, mx, sm, ob, ab, bias1, bias2, bias2f,
     load, in_send, in_recv, q_send, q_recv, z_send, z_recv, zb_send, zb_recv, zc_send, zc_recv, o_send, o_recv, d_send, d_recv,
     ) = refs[PARTS:]
     res, dim = DILATION_THREE, q_ref.shape[-1]
@@ -221,10 +221,6 @@
         bias2.shape, shifted(place_two(ROWS_TWO), ROWS_TWO * RATIO), place_two(2 * ROWS_TWO), ROWS_TWO,
         WINDOW_TWO // DILATION_TWO, has_prev,
     )
-    _, bias3[...] = bias_of(
-        bias3.shape, lambda i: (i + rows, i), lambda i: (i, i), rows, WINDOW_THREE // DILATION_THREE, has_prev
-    )
-
     pl.semaphore_wait(barrier, group + jnp.where(has_prev, 1, 0) + jnp.where(has_next, 1, 0))
 
     @pl.when(has_next)
@@ -285,12 +281,20 @@
         block = tuple(x[part, at, :].reshape(-1, dim) for x, at in ((qb, own), (kb, near_rows), (vb, near_rows)))
         return block + (bias[...],), keep
 
+    ahead = [lax.broadcasted_iota(jnp.int32, (rows, rows), i) for i in (1, 0)]
+    ahead = ahead[0] - ahead[1]
+    gate = jnp.where(has_prev, 0, rows)
+
+    def band(x):
+        earlier = jnp.where(ahead >= gate, x[:, :rows], -jnp.inf)
+        return jnp.concatenate([earlier, jnp.where(ahead <= 0, x[:, rows:], -jnp.inf)], axis=1)
+
     def three(x):
         def keep(found):
             weighted, _, total = merge((x,), *found)
             ob[x] = (weighted / total).astype(ob.dtype)
 
-        return (qb[x], kb[x], vb[x], bias3[...]), keep
+        return (qb[x], kb[x], vb[x], band), keep
 
     def run(*groups):
         parts = [item for items, _ in groups for item in items]
@@ -340,7 +344,6 @@
         arrival(2, d).wait_recv()
     for d, b in zip(near, (soon, near_far)):
         run((inners(d) + [one(b * steps)], nothing))
-    run(([two(s, soon) for s in range(CHUNKS)], nothing))
 
     @pl.when(has_prev)
     def _():
@@ -356,7 +359,7 @@
             for d in far if first == s else ():
                 arrival(2, d, i).wait_recv()
                 found += inners(d, i) + [one(member(d) * steps, jnp.where(member(d) == 0, 1, 0), i)]
-        return found + [two(s, b) for b in later]
+        return found + [two(s, b) for b in (soon, *later)]
 
 
     head = tp * group + mine
@@ -456,12 +459,11 @@
         for u in units[1:]:
             from_prev(*[onward_late(x, u) for x in (0, 1)])
             run((threes(u), hand_out(u)))
-        if s == 2:
-            hand_over(0)
     loads[3].wait()
-    for u in range(1, len(UNITS)):
+    for u in range(len(UNITS)):
         hand_over(u)
-        project(u - 1)
+        if u:
+            project(u - 1)
     project(len(UNITS) - 1)
 
     per = piece // PARTS
@@ -503,7 +505,7 @@
     piece = tokens // res
     rows = group * piece
     assert group == 4 and piece > ROWS_ONE
-    assert group * tokens == WINDOW_THREE and lax.axis_size("sp") % group == 0 and lax.axis_size("tp") == 2
+    assert group * tokens == WINDOW_THREE and WINDOW_THREE // DILATION_THREE == rows and lax.axis_size("sp") % group == 0 and lax.axis_size("tp") == 2
 
     low, full = jnp.bfloat16, jnp.float32
     dma = pltpu.SemaphoreType.DMA
@@ -533,7 +535,6 @@
             pltpu.VMEM((2, res * ROWS_ONE, 2 * res * ROWS_ONE), full),
             pltpu.VMEM((RATIO * ROWS_TWO, 2 * RATIO * ROWS_TWO), full),
             pltpu.VMEM((RATIO * ROWS_TWO, 2 * RATIO * ROWS_TWO), full),
-            pltpu.VMEM((rows, 2 * rows), full),
             dma((4,)),
             dma((3, group)), dma((3, group)),
             dma((len(QUERY_PARTS),)), dma((len(QUERY_PARTS),)),

time: 35.9 us -> 35.3 us (0.983)
  Pallas kernels: 34.4 us -> 34 us
    pallas_call x1, Pallas kernels: 34.4 us -> 34 us  [local(): pl.pallas_call(functools.partial(kernel, group), out_shape=[jax.ShapeDtyp...]
where the time goes in v4:
time: 35.3 us; the launch traced here: 35 us
  Pallas kernels  34 us (96%)
  other arithmetic  1.04 us (3%)
    pallas_call x1, Pallas kernels, local(): pl.pallas_call(functools.partial(kernel, group), out_shape=[jax.ShapeDtyp...  34 us
    concatenate x1, other arithmetic, local(): return jnp.concatenate(mixed, axis=0)  1.04 us

profile of v4, /device:TPU:0, one launch (start us, length us, event | category | flops | bytes accessed | tf_op | source)
XLA Modules:
  0.0 35.0 jit_solution(14422344739554943001)
XLA Ops:
  0.0 34.0 %shard_map.46 = (bf16[256,1024]{1,0:T(8,128)(2,1)S(1)}, bf16[256,1024]{1,0:T(8,128)(2,1)S(1)}) custom-call(bf16[512,4,128]{2,1,0:T(4,128)(2,1)} %q_hbm.1, bf16[512,4,128]{2,1,0:T(4,128)(2,1)} %k_hbm.1, bf16[512,4,128]{2,1,0:T(4,128)(2,1)} %v_hbm.1, bf16[1024,1024]{1,0:T(8,128)(2,1)} %w_hbm.1), custom_call_target="tpu_custom_call" | custom-call | tf_op jit(solution)/shard_map/pallas_call | solution.py:514
  34.0 1.0 %pad_maximum_fusion = bf16[512,1024]{1,0:T(8,128)(2,1)} fusion(bf16[256,1024]{1,0:T(8,128)(2,1)S(1)} %get-tuple-element.8, bf16[256,1024]{1,0:T(8,128)(2,1)S(1)} %get-tuple-element.7), kind=kLoop, calls=%fused_computation | loop fusion | flops 2097152 | bytes 2097152 | tf_op jit(solution)/shard_map/concatenate | solution.py:551
